TPU v7x, 32 devices: a whole 2x2x4 slice. The times are simulated.
32 devices in a mesh: grp: 2 (over x), ep: 8 (over z, y), tp: 2 (over core).
Axes of the slice: x: 2, y: 2, z: 4, core: 2. Of those that a mesh axis runs over, the one named last changes fastest.
Arguments:
- tokens: bfloat16 [3072, 2048], P(('grp', 'ep'), 'tp'), parts along dimension 0, may hold values from -10 to 10
- gain_in: float32 [2048], replicated, may hold values from 0.1 to 1.9
- gain_out: float32 [2048], replicated, may hold values from 0.1 to 1.9
- expert_ids: int32 [3072, 2], P(('grp', 'ep')), parts along dimension 0, may hold values from 0 to 3, all different within a row; in each aligned block of 192 rows (0 to 191, 192 to 383, ...) at most 144 rows name the same one
- route_weight: float32 [3072, 2], P(('grp', 'ep')), parts along dimension 0, may hold values from 0.1 to 1
- gate_weight: bfloat16 [8, 2048, 1792], P('ep', None, 'tp'), may hold values from -0.125 to 0.125
- up_weight: bfloat16 [8, 2048, 1792], P('ep', None, 'tp'), may hold values from -0.125 to 0.125
- down_weight: bfloat16 [8, 1792, 2048], P('ep', 'tp'), may hold values from -1 to 1
Outputs:
- layer_out: bfloat16 [3072, 2048], P(('grp', 'ep'), 'tp'), parts along dimension 0
There are 2 independent parts, one for each index of `grp`. A program takes and returns all parts, laid end to end along the dimension named above; an argument that names none is the same for every part. Nothing has to cross between parts.
Inputs may be any that keep to these rules, and one draw needn't show every extreme that they name: `expert_ids`: each row names 2 different experts. Among the tokens of one index of ep no expert is named more than 144 times, a bound that some block reaches.
All inputs are finite; a program needn't handle non-finite values.
Results may differ from a plain program's by a relative error of at most 0.0077.
Values may be sent and summed in bfloat16 or wider, within the bound.
A program may use at most 64 MiB of HBM per device.

v0:
```python
import jax
import jax.numpy as jnp
from jax import lax
from jax.sharding import PartitionSpec as P

norm_eps = 1e-06


def shards(
    tokens, gain_in, gain_out, expert_ids, route_weight, gate_weight, up_weight, down_weight
):
    tok_rows, half_width = tokens.shape
    full_width = 2 * half_width
    expert_count = lax.axis_size("ep") // 2
    picks = expert_ids.shape[1]
    capacity = tok_rows * picks * 3 // (2 * expert_count)
    own_cols = lax.axis_index("tp") * half_width
    own_float = tokens.astype(jnp.float32)
    squares = lax.psum(jnp.sum(own_float * own_float, axis=1), "tp")
    factor = lax.rsqrt(squares / full_width + norm_eps)[:, None]
    own_gain = lax.dynamic_slice_in_dim(gain_in, own_cols, half_width)
    normed = (own_float * factor * own_gain).astype(jnp.bfloat16)
    sent_width = normed.shape[1]
    flat_ids = expert_ids.reshape(-1)
    onehot = (flat_ids[:, None] == jnp.arange(expert_count, dtype=jnp.int32)[None, :]).astype(
        jnp.int32
    )
    before = jnp.cumsum(onehot, axis=0) - onehot
    targets = flat_ids * capacity + jnp.sum(before * onehot, axis=1)
    per_token = targets.reshape(tok_rows, picks)
    slot_rows = jnp.arange(expert_count * capacity, dtype=jnp.int32)[:, None]
    placing = jnp.zeros((expert_count * capacity, tok_rows), jnp.bfloat16)
    for which in range(picks):
        placing = placing + (slot_rows == per_token[None, :, which]).astype(jnp.bfloat16)
    packed = jnp.dot(placing, normed, preferred_element_type=jnp.float32).astype(jnp.bfloat16)
    stacked = packed.reshape(expert_count, 1, capacity, sent_width)
    outgoing = jnp.broadcast_to(stacked, (expert_count, 2, capacity, sent_width)).reshape(
        2 * expert_count, capacity, sent_width
    )
    arrived = lax.all_to_all(outgoing, "ep", split_axis=0, concat_axis=0, tiled=True)
    arrived = lax.all_gather(arrived, "tp", axis=2, tiled=True)
    sources = arrived.shape[0]
    gathered = arrived.reshape(sources * capacity, full_width)
    gate_pre = jnp.dot(gathered, gate_weight[0], preferred_element_type=jnp.float32)
    up_pre = jnp.dot(gathered, up_weight[0], preferred_element_type=jnp.float32)
    hidden = (jax.nn.silu(gate_pre) * up_pre).astype(jnp.bfloat16)
    partial_value = jnp.dot(hidden, down_weight[0], preferred_element_type=jnp.float32).astype(
        jnp.bfloat16
    )
    partial_value = partial_value.reshape(sources, capacity, full_width)
    half_sum = lax.psum_scatter(partial_value, "tp", scatter_dimension=2, tiled=True).astype(
        jnp.float32
    )
    returned = lax.all_to_all(
        half_sum.astype(jnp.bfloat16), "ep", split_axis=0, concat_axis=0, tiled=True
    )
    merged = jnp.sum(
        returned.reshape(expert_count, 2, capacity, half_width).astype(jnp.float32), axis=1
    )
    merged = merged.reshape(expert_count * capacity, half_width)
    picked = jnp.take(merged, targets, axis=0).reshape(tok_rows, picks, half_width)
    routed = jnp.sum(picked * route_weight[:, :, None], axis=1)
    squares_out = lax.psum(jnp.sum(routed * routed, axis=1), "tp")
    factor_out = lax.rsqrt(squares_out / full_width + norm_eps)[:, None]
    own_gain_out = lax.dynamic_slice_in_dim(gain_out, own_cols, half_width)
    return (routed * factor_out * own_gain_out).astype(jnp.bfloat16)


def solution(mesh):
    in_specs = (
        P(("grp", "ep"), "tp"),
        P(),
        P(),
        P(("grp", "ep"), None),
        P(("grp", "ep"), None),
        P("ep", None, "tp"),
        P("ep", None, "tp"),
        P("ep", "tp", None),
    )
    out_specs = P(("grp", "ep"), "tp")
    return jax.shard_map(shards, mesh=mesh, in_specs=in_specs, out_specs=out_specs, check_vma=False)
```

profile of v0, /device:TPU:0, one launch (start us, length us, event | category | flops | bytes accessed | tf_op | source)
XLA Modules:
  0.0 206.4 jit_solution(4754429153648851285)
XLA Ops:
  6.5 0.0 all-gather.2.cloned.1.call-start
  6.5 0.8 copy.19
  7.3 0.1 eq.56
  7.5 0.1 reshape.88
  7.6 1.2 reduce-window.6
  8.9 0.2 slice_reduce_fusion
  9.1 0.2 reduce-window.9
  9.3 0.1 add_bitcast_fusion
  9.4 0.1 reduce_sum.50
  9.5 0.1 copy.21
  9.6 0.7 compare_and_fusion
  10.3 1.2 fusion.7
  11.5 2.6 %psum.14 = f32[192]{0:T(256)S(1)} all-reduce(f32[192]{0:T(256)S(1)} %fusion.7), channel_id=1, replica_groups=mesh['grp'=2,'ep'=8,'tp'=2] {'tp'}, use_global_device_ids=true, to_apply=%region_4.5 | all-reduce | flops 192 | bytes 1536 | tf_op jit(solution)/shard_map/psum | solution.py:19
  14.1 0.7 dynamic_slice.6
  14.8 1.6 convolution_convert_fusion.1
  16.4 0.3 broadcast_in_dim.26
  16.7 61.2 %all_to_all.10 = bf16[8,144,1024]{2,1,0:T(8,128)(2,1)} all-to-all(bf16[8,144,1024]{2,1,0:T(8,128)(2,1)S(1)} %bitcast.44), channel_id=1, replica_groups=mesh['grp'=2,'ep'=8,'tp'=2] {'ep'}, dimensions={0} | all-to-all | bytes 4718592 | tf_op jit(solution)/shard_map/all_to_all | solution.py:40
  77.9 0.0 all-gather.2.cloned.1.call-update
  77.9 0.0 reduce-scatter.2.cloned.1.call-start
  77.9 13.6 %all-gather.2.cloned.1.call-done = bf16[8,144,2048]{2,1,0:T(8,128)(2,1)} async-done(((bf16[8,144,1024]{2,1,0:T(8,128)(2,1)}), bf16[8,144,2048]{2,1,0:T(8,128)(2,1)}) %all-gather.2.cloned.1.call-update) | async-done | bytes 4718608 | tf_op jit(solution)/shard_map/all_gather | solution.py:41
  91.5 0.0 copy-start.2
  91.5 0.0 copy-start.3
  91.5 8.1 %fusion.2 = f32[1152,896]{1,0:T(8,128)S(1)} fusion(bf16[1152,2048]{1,0:T(8,128)(2,1)} %bitcast.50, bf16[1,2048,896]{2,1,0:T(8,128)(2,1)} %param.13), kind=kOutput, calls=%fused_computation.6 | convolution fusion | flops 4227858432 | bytes 12517376 | tf_op jit(solution)/shard_map/dot_general | solution.py:44
  99.7 0.0 copy-done.2
  99.7 0.0 copy-done.3
  99.7 0.0 copy-start.4
  99.7 5.3 %fusion.4 = bf16[1152,896]{1,0:T(8,128)(2,1)S(1)} fusion(bf16[1152,2048]{1,0:T(8,128)(2,1)S(1)} %bitcast.51, bf16[1,2048,896]{2,1,0:T(8,128)(2,1)S(1)} %copy-done.3, f32[1152,896]{1,0:T(8,128)S(1)} %fusion.2), kind=kOutput, calls=%fused_computation.8 | convolution fusion | flops 4234051584 | bytes 14581760 | tf_op jit(solution)/shard_map/dot_general | solution.py:45
  105.0 0.0 copy-done.4
  105.0 6.7 %convolution_convert_fusion = bf16[1152,2048]{1,0:T(8,128)(2,1)} fusion(bf16[1152,896]{1,0:T(8,128)(2,1)S(1)} %fusion.4, bf16[1,896,2048]{2,1,0:T(8,128)(2,1)S(1)} %copy-done.4), kind=kOutput, calls=%fused_computation.1 | convolution fusion | flops 4230217728 | bytes 10452992 | tf_op jit(solution)/shard_map/dot_general | solution.py:47
  111.8 0.0 copy-start
  111.8 0.0 copy-start.1
  111.8 0.0 reduce-scatter.2.cloned.1.call-update
  111.8 13.7 %reduce-scatter.2.cloned.1.call-done = bf16[8,144,1024]{2,1,0:T(8,128)(2,1)} async-done(((bf16[8,144,2048]{2,1,0:T(8,128)(2,1)}), bf16[8,144,1024]{2,1,0:T(8,128)(2,1)}) %reduce-scatter.2.cloned.1.call-update) | async-done | bytes 2359312 | tf_op jit(solution)/shard_map/reduce_scatter | solution.py:51
  125.5 5.9 %all-to-all-start.1 = ((bf16[8,144,1024]{2,1,0:T(8,128)(2,1)}), bf16[8,144,1024]{2,1,0:T(8,128)(2,1)}, u32[]{:S(2)}, u32[]{:S(2)}) async-start(bf16[8,144,1024]{2,1,0:T(8,128)(2,1)} %reduce-scatter.2.cloned.1.call-done), calls=%async_computation.2 | async-start | bytes 4718592 | tf_op jit(solution)/shard_map/all_to_all | solution.py:54
  131.4 0.0 copy-done
  131.4 0.1 copy.23
  131.5 0.1 mul.90
  131.7 0.2 copy.22
  131.8 0.0 copy-done.1
  131.8 0.1 copy.24
  132.0 53.6 %all-to-all-done.1 = bf16[8,144,1024]{2,1,0:T(8,128)(2,1)} async-done(((bf16[8,144,1024]{2,1,0:T(8,128)(2,1)}), bf16[8,144,1024]{2,1,0:T(8,128)(2,1)}, u32[]{:S(2)}, u32[]{:S(2)}) %all-to-all-start.1) | async-done | bytes 2359328 | tf_op jit(solution)/shard_map/all_to_all | solution.py:54
  185.7 2.5 %convert_reduce_fusion = f32[4,144,1024]{2,1,0:T(8,128)S(1)} fusion(bf16[8,144,1024]{2,1,0:T(8,128)(2,1)} %all-to-all-done.1), kind=kLoop, calls=%fused_computation.2 | loop fusion | flops 1769472 | bytes 4718592 | tf_op jit(solution)/shard_map/reduce_sum | solution.py:57
  188.1 2.5 %gather_fusion = f32[384,1024]{1,0:T(8,128)} fusion(f32[576,1024]{1,0:T(8,128)S(1)} %bitcast.43, s32[1024]{0:T(1024)S(1)} %pad_clamp_fusion), kind=kCustom, calls=%fused_computation | custom fusion | bytes 3147264 | tf_op jit(solution)/shard_map/jit(_take)/gather | solution.py:61
  190.6 0.0 dynamic-slice-start
  190.6 2.2 %gather.7 = f32[192,2,1024]{2,1,0:T(2,128)S(1)} reshape(f32[384,1024]{1,0:T(8,128)} %gather_fusion) | data formatting | bytes 3145728 | tf_op jit(solution)/shard_map/jit(_take)/gather | solution.py:61
  192.9 3.1 %multiply_reduce_fusion = f32[192,1024]{1,0:T(8,128)S(1)} fusion(f32[192,2,1024]{2,1,0:T(2,128)S(1)} %gather.7, pred[192,2]{1,0:T(8,128)(4,1)S(1)} %copy.22, f32[192,2]{1,0:T(8,128)S(1)} %copy.24), kind=kLoop, calls=%fused_computation.9 | loop fusion | flops 983040 | bytes 2361216 | tf_op jit(solution)/shard_map/reduce_sum | solution.py:62
  196.0 0.1 multiply_reduce_fusion.1
  196.1 2.5 %psum.15 = f32[192]{0:T(256)S(1)} all-reduce(f32[192]{0:T(256)S(1)} %multiply_reduce_fusion.1), channel_id=1, replica_groups=mesh['grp'=2,'ep'=8,'tp'=2] {'tp'}, use_global_device_ids=true, to_apply=%region_9.10 | all-reduce | flops 192 | bytes 1536 | tf_op jit(solution)/shard_map/psum | solution.py:63
  198.6 0.0 dynamic-slice-done
  198.6 0.9 multiply_convert_fusion
  (8 shorter events, 0.1 us)
Async XLA Ops:
  6.5 85.0 %all-gather.2.cloned.1.call-start = ((), (), s32[]{:S(2)}) async-start(), calls=%async_computation.3 | async-start | bytes 7077888 | tf_op jit(solution)/shard_map/all_gather | solution.py:41
  77.9 47.6 %reduce-scatter.2.cloned.1.call-start = ((), (), s32[]{:S(2)}) async-start(), calls=%async_computation.4 | async-start | bytes 7077888 | tf_op jit(solution)/shard_map/reduce_scatter | solution.py:51
  91.5 8.1 %copy-start.2 = (bf16[8,144,2048]{2,1,0:T(8,128)(2,1)S(1)}, bf16[8,144,2048]{2,1,0:T(8,128)(2,1)}, u32[]{:S(2)}) copy-start(bf16[8,144,2048]{2,1,0:T(8,128)(2,1)} %all-gather.2.cloned.1.call-done) | copy-start | bytes 14155780
  91.5 8.1 %copy-start.3 = (bf16[1,2048,896]{2,1,0:T(8,128)(2,1)S(1)}, bf16[1,2048,896]{2,1,0:T(8,128)(2,1)}, u32[]{:S(2)}) copy-start(bf16[1,2048,896]{2,1,0:T(8,128)(2,1)} %param.14) | copy-start | bytes 11010052
  99.7 5.3 %copy-start.4 = (bf16[1,896,2048]{2,1,0:T(8,128)(2,1)S(1)}, bf16[1,896,2048]{2,1,0:T(8,128)(2,1)}, u32[]{:S(2)}) copy-start(bf16[1,896,2048]{2,1,0:T(8,128)(2,1)} %param.15) | copy-start | bytes 11010052
  111.8 19.6 %copy-start = (s32[192,2]{0,1:T(2,128)S(1)}, s32[192,2]{0,1:T(2,128)}, u32[]{:S(2)}) copy-start(s32[192,2]{0,1:T(2,128)} %param.11) | copy-start | bytes 4612
  111.8 20.1 %copy-start.1 = (f32[192,2]{0,1:T(2,128)S(1)}, f32[192,2]{0,1:T(2,128)}, u32[]{:S(2)}) copy-start(f32[192,2]{0,1:T(2,128)} %param.12) | copy-start | bytes 4612
  125.5 60.2 %all-to-all-start.1 = ((bf16[8,144,1024]{2,1,0:T(8,128)(2,1)}), bf16[8,144,1024]{2,1,0:T(8,128)(2,1)}, u32[]{:S(2)}, u32[]{:S(2)}) async-start(bf16[8,144,1024]{2,1,0:T(8,128)(2,1)} %reduce-scatter.2.cloned.1.call-done), calls=%async_computation.2 | async-start | bytes 4718592 | tf_op jit(solution)/shard_map/all_to_all | solution.py:54
  190.6 8.0 %dynamic-slice-start = ((f32[2048]{0:T(1024)}, s32[]{:T(128)}), f32[1024]{0:T(1024)S(1)}, s32[]{:S(2)}) async-start(f32[2048]{0:T(1024)} %param.10, s32[]{:T(128)} %select_n.27), calls=%async_computation.5 | async-start | bytes 8704 | tf_op jit(solution)/shard_map/dynamic_slice | solution.py:65
Sparse Core Ops, SparseCore 0:
  78.0 13.4 all-gather.1
  111.9 13.5 reduce-scatter.1
where the time goes:
time: 207 us; the launch traced here: 206 us
  waiting for transfers between devices  81 us (39%)
  blocking collectives  66.3 us (32%)
  matrix products  21.7 us (10%)
  between operations  13.6 us (7%)
  other arithmetic  10 us (5%)
  local copies, waits for them, and re-layouts  7.8 us (4%)
  starting transfers between devices  5.94 us (3%)
    all_to_all x1, blocking collectives, shards(): lax.all_to_all(outgoing, 'ep', split_axis=0, concat_axis=0, tiled=True)  61.2 us
    all_to_all x1, waiting for transfers between devices, shards(): lax.all_to_all(half_sum.astype(jnp.bfloat16), 'ep', split_axis=0, concat_...  53.6 us
    reduce_scatter x1, waiting for transfers between devices, shards(): lax.psum_scatter(partial_value, 'tp', scatter_dimension=2, tiled=True)  13.7 us
    all_gather x1, waiting for transfers between devices, shards(): arrived = lax.all_gather(arrived, 'tp', axis=2, tiled=True)  13.6 us
    dot_general x1, matrix products, shards(): jnp.dot(gathered, gate_weight[0], preferred_element_type=jnp.float32)  8.11 us
    dot_general x1, matrix products, shards(): jnp.dot(hidden, down_weight[0], preferred_element_type=jnp.float32)  6.72 us
    all_to_all x1, starting transfers between devices, shards(): lax.all_to_all(half_sum.astype(jnp.bfloat16), 'ep', split_axis=0, concat_...  5.9 us
    dot_general x1, matrix products, shards(): up_pre = jnp.dot(gathered, up_weight[0], preferred_element_type=jnp.float32)  5.32 us
  transfers between devices with their start and end apart: 3, of which 3 were waited for; matrix products, arithmetic and copies ran while one was open for 0% of the time, Pallas kernels for 0%

commit v1 on v0

--- a/solution.py
+++ b/solution.py
@@ -1,12 +1,16 @@
+import functools
+
 import jax
 import jax.numpy as jnp
 from jax import lax
+from jax.experimental import pallas as pl
+from jax.experimental.pallas import tpu as pltpu
 from jax.sharding import PartitionSpec as P
 
 norm_eps = 1e-06
 
 
-def shards(
+def plain(
     tokens, gain_in, gain_out, expert_ids, route_weight, gate_weight, up_weight, down_weight
 ):
     tok_rows, half_width = tokens.shape
@@ -66,6 +70,365 @@
     return (routed * factor_out * own_gain_out).astype(jnp.bfloat16)
 
 
+MESH = pl.DeviceIdType.MESH
+
+
+def fused(
+    experts,
+    cap,
+    tok_ref,
+    gain_in_ref,
+    gain_out_ref,
+    ids_ref,
+    route_ref,
+    gate_hbm,
+    up_hbm,
+    down_hbm,
+    out_ref,
+    packed,
+    rows,
+    parts,
+    peer_parts,
+    kept,
+    crossing,
+    crossed,
+    leaving,
+    home,
+    gate_up,
+    down,
+    sums,
+    peer_sums,
+    total,
+    w_sem,
+    sq_send,
+    sq_recv,
+    line_send,
+    line_recv,
+    core_send,
+    core_recv,
+    pair_send,
+    pair_recv,
+    relay_send,
+    relay_recv,
+    part_send,
+    part_recv,
+    cross_send,
+    cross_recv,
+    home_send,
+    home_recv,
+):
+    tok_rows, width = tok_ref.shape
+    hidden_width = down.shape[0]
+    place = lax.axis_index("ep")
+    core = lax.axis_index("tp")
+    half = place % 2
+    mine = place // 2
+    partner = place + 1 - 2 * half
+    other = 1 - core
+    own_cols = pl.ds(pl.multiple_of(core * width, 128), width)
+    other_cols = pl.ds(pl.multiple_of(other * width, 128), width)
+
+    def on_line(step):
+        return 2 * ((mine + step) % experts) + half
+
+    loads = [
+        pltpu.make_async_copy(gate_hbm.at[0], gate_up.at[:, pl.ds(0, hidden_width)], w_sem.at[0]),
+        pltpu.make_async_copy(
+            up_hbm.at[0], gate_up.at[:, pl.ds(hidden_width, hidden_width)], w_sem.at[1]
+        ),
+        pltpu.make_async_copy(down_hbm.at[0], down, w_sem.at[2]),
+    ]
+    barrier = pltpu.get_barrier_semaphore()
+    pl.semaphore_signal(barrier, inc=1, device_id={"tp": other}, device_id_type=MESH)
+    pl.semaphore_signal(barrier, inc=1, device_id={"ep": partner}, device_id_type=MESH)
+    for step in range(1, experts):
+        pl.semaphore_signal(barrier, inc=1, device_id={"ep": on_line(step)}, device_id_type=MESH)
+    for load in loads:
+        load.start()
+
+    def remote(source, target, send, recv, device):
+        return pltpu.make_async_remote_copy(
+            src_ref=source,
+            dst_ref=target,
+            send_sem=send,
+            recv_sem=recv,
+            device_id=device,
+            device_id_type=MESH,
+        )
+
+    def sum_copy(which):
+        return remote(
+            sums.at[which], peer_sums.at[which], sq_send.at[which], sq_recv.at[which], {"tp": other}
+        )
+
+    def line_copy(step):
+        back = experts - step
+        return remote(
+            packed.at[step],
+            rows.at[back, 0, :, own_cols],
+            line_send.at[back],
+            line_recv.at[back],
+            {"ep": on_line(step)},
+        )
+
+    def core_copy(d):
+        view = rows.at[d, 0, :, own_cols]
+        return remote(view, view, core_send.at[d], core_recv.at[d], {"tp": other})
+
+    def core_arrival(d):
+        view = rows.at[d, 0, :, other_cols]
+        return remote(view, view, core_send.at[d], core_recv.at[d], {"tp": other})
+
+    def pair_copy(d):
+        return remote(
+            rows.at[d, 0, :, own_cols],
+            rows.at[d, 1, :, own_cols],
+            pair_send.at[d],
+            pair_recv.at[d],
+            {"ep": partner},
+        )
+
+    def relay_copy(d):
+        view = rows.at[d, 1, :, own_cols]
+        return remote(view, view, relay_send.at[d], relay_recv.at[d], {"tp": other})
+
+    def relay_arrival(d):
+        view = rows.at[d, 1, :, other_cols]
+        return remote(view, view, relay_send.at[d], relay_recv.at[d], {"tp": other})
+
+    def part_copy(d):
+        return remote(
+            parts.at[d, :, :, other_cols],
+            peer_parts.at[d],
+            part_send.at[d],
+            part_recv.at[d],
+            {"tp": other},
+        )
+
+    def cross_copy(d):
+        return remote(
+            crossing.at[d], crossed.at[d], cross_send.at[d], cross_recv.at[d], {"ep": partner}
+        )
+
+    def home_copy(d):
+        back = experts - d
+        return remote(
+            leaving.at[d], home.at[back], home_send.at[back], home_recv.at[back], {"ep": on_line(d)}
+        )
+
+    own_float = tok_ref[...].astype(jnp.float32)
+    sums[0] = jnp.broadcast_to(
+        jnp.sum(own_float * own_float, axis=1, keepdims=True), (tok_rows, 128)
+    )
+    pl.semaphore_wait(barrier, experts + 1)
+    sum_copy(0).start()
+
+    lead = max(8, experts)
+    names = lax.broadcasted_iota(jnp.int32, (lead, tok_rows), 0)
+    first = names == ids_ref[0:1, :]
+    second = names == ids_ref[1:2, :]
+    either = (first.astype(jnp.float32) + second.astype(jnp.float32)).astype(jnp.bfloat16)
+    earlier = (
+        lax.broadcasted_iota(jnp.int32, (tok_rows, tok_rows), 0)
+        < lax.broadcasted_iota(jnp.int32, (tok_rows, tok_rows), 1)
+    ).astype(jnp.float32).astype(jnp.bfloat16)
+    before = jnp.dot(either, earlier, preferred_element_type=jnp.float32)
+    slot_one = jnp.sum(jnp.where(first, before, 0.0), axis=0, keepdims=True).astype(jnp.int32)
+    slot_two = jnp.sum(jnp.where(second, before, 0.0), axis=0, keepdims=True).astype(jnp.int32)
+    target_one = ids_ref[0:1, :] * cap + slot_one
+    target_two = ids_ref[1:2, :] * cap + slot_two
+    slot_rows = lax.broadcasted_iota(jnp.int32, (cap, tok_rows), 0)
+
+    def hits(step):
+        base = ((mine + step) % experts) * cap
+        return slot_rows + base == target_one, slot_rows + base == target_two
+
+    sum_copy(0).wait_recv()
+    squares = sums[0] + peer_sums[0]
+    factor = lax.rsqrt(squares[:, 0:1] / (2 * width) + norm_eps)
+    normed = (own_float * factor * gain_in_ref[...]).astype(jnp.bfloat16)
+
+    def pack(step):
+        one, two = hits(step)
+        placing = (one.astype(jnp.float32) + two.astype(jnp.float32)).astype(jnp.bfloat16)
+        return jnp.dot(placing, normed, preferred_element_type=jnp.float32).astype(jnp.bfloat16)
+
+    rows[0, 0, :, own_cols] = pack(0)
+    pair_copy(0).start()
+    core_copy(0).start()
+    for step in range(experts - 1, 0, -1):
+        packed[step] = pack(step)
+        line_copy(step).start()
+
+    def relay_line(d):
+        line_copy(experts - d).wait_recv()
+        pair_copy(d).start()
+        core_copy(d).start()
+
+    def relay_pair(d):
+        pair_copy(d).wait_recv()
+        relay_copy(d).start()
+
+    def compute(d):
+        core_arrival(d).wait_recv()
+        relay_arrival(d).wait_recv()
+        block = rows[d].reshape(2 * cap, 2 * width)
+        pre = jnp.dot(block, gate_up[...], preferred_element_type=jnp.float32)
+        gate_pre = pre[:, :hidden_width]
+        hidden = (gate_pre / (1.0 + jnp.exp(-gate_pre)) * pre[:, hidden_width:]).astype(
+            jnp.bfloat16
+        )
+        partial = jnp.dot(hidden, down[...], preferred_element_type=jnp.float32)
+        parts[d] = partial.astype(jnp.bfloat16).reshape(2, cap, 2 * width)
+        part_copy(d).start()
+
+    def cross(d):
+        part_copy(d).wait_recv()
+        crossing[d] = (
+            parts[d, 1, :, own_cols].astype(jnp.float32) + peer_parts[d, 1].astype(jnp.float32)
+        ).astype(jnp.bfloat16)
+        cross_copy(d).start()
+        kept[d] = parts[d, 0, :, own_cols].astype(jnp.float32) + peer_parts[d, 0].astype(
+            jnp.float32
+        )
+
+    def send_home(d):
+        cross_copy(d).wait_recv()
+        return (kept[d] + crossed[d].astype(jnp.float32)).astype(jnp.bfloat16)
+
+    relay_pair(0)
+    for load in loads:
+        load.wait()
+
+    def step_of(d, carry):
+        @pl.when(d + 1 < experts)
+        def _():
+            relay_line(d + 1)
+
+        compute(d)
+
+        @pl.when(d + 1 < experts)
+        def _():
+            relay_pair(d + 1)
+
+        cross(d)
+
+        @pl.when(d == 1)
+        def _():
+            home[0] = send_home(0)
+
+        @pl.when(d > 1)
+        def _():
+            leaving[d - 1] = send_home(d - 1)
+            home_copy(d - 1).start()
+
+        return carry
+
+    lax.fori_loop(0, experts, step_of, 0)
+    leaving[experts - 1] = send_home(experts - 1)
+    home_copy(experts - 1).start()
+
+    def combine(step):
+        one, two = hits(step)
+        mix = jnp.where(one, route_ref[0:1, :], 0.0) + jnp.where(two, route_ref[1:2, :], 0.0)
+        high = mix.astype(jnp.bfloat16)
+        low = (mix - high.astype(jnp.float32)).astype(jnp.bfloat16)
+        dims = (((0,), (0,)), ((), ()))
+        return lax.dot_general(
+            high, home[step], dims, preferred_element_type=jnp.float32
+        ) + lax.dot_general(low, home[step], dims, preferred_element_type=jnp.float32)
+
+    total[...] = combine(0)
+    for step in range(experts - 1, 0, -1):
+        home_copy(experts - step).wait_recv()
+        total[...] += combine(step)
+    routed = total[...]
+    sums[1] = jnp.broadcast_to(jnp.sum(routed * routed, axis=1, keepdims=True), (tok_rows, 128))
+    sum_copy(1).start()
+    sum_copy(1).wait_recv()
+    squares_out = sums[1] + peer_sums[1]
+    factor_out = lax.rsqrt(squares_out[:, 0:1] / (2 * width) + norm_eps)
+    out_ref[...] = (total[...] * factor_out * gain_out_ref[...]).astype(jnp.bfloat16)
+
+    sum_copy(0).wait_send()
+    sum_copy(1).wait_send()
+
+    def drain(d, carry):
+        core_copy(d).wait_send()
+        pair_copy(d).wait_send()
+        relay_copy(d).wait_send()
+        part_copy(d).wait_send()
+        cross_copy(d).wait_send()
+
+        @pl.when(d > 0)
+        def _():
+            line_copy(d).wait_send()
+            home_copy(d).wait_send()
+
+        return carry
+
+    lax.fori_loop(0, experts, drain, 0)
+
+
+def layer(
+    tokens, gain_in, gain_out, expert_ids, route_weight, gate_weight, up_weight, down_weight
+):
+    tok_rows, width = tokens.shape
+    experts = lax.axis_size("ep") // 2
+    picks = expert_ids.shape[1]
+    cap = tok_rows * picks * 3 // (2 * experts)
+    hidden_width = gate_weight.shape[2]
+    if picks != 2 or experts < 2 or cap % 16 or width % 128 or hidden_width % 128:
+        return plain(
+            tokens, gain_in, gain_out, expert_ids, route_weight, gate_weight, up_weight, down_weight
+        )
+    own = lax.axis_index("tp") * width
+    own_gain_in = lax.dynamic_slice_in_dim(gain_in, own, width)[None, :]
+    own_gain_out = lax.dynamic_slice_in_dim(gain_out, own, width)[None, :]
+    vmem = pl.BlockSpec(memory_space=pltpu.VMEM)
+    hbm = pl.BlockSpec(memory_space=pl.ANY)
+    bf16, f32 = jnp.bfloat16, jnp.float32
+    lines = [pltpu.SemaphoreType.DMA((experts,))] * 14
+    return pl.pallas_call(
+        functools.partial(fused, experts, cap),
+        out_shape=jax.ShapeDtypeStruct((tok_rows, width), bf16),
+        in_specs=[vmem] * 5 + [hbm] * 3,
+        out_specs=vmem,
+        scratch_shapes=[
+            pltpu.VMEM((experts, cap, width), bf16),
+            pltpu.VMEM((experts, 2, cap, 2 * width), bf16),
+            pltpu.VMEM((experts, 2, cap, 2 * width), bf16),
+            pltpu.VMEM((experts, 2, cap, width), bf16),
+            pltpu.VMEM((experts, cap, width), f32),
+            pltpu.VMEM((experts, cap, width), bf16),
+            pltpu.VMEM((experts, cap, width), bf16),
+            pltpu.VMEM((experts, cap, width), bf16),
+            pltpu.VMEM((experts, cap, width), bf16),
+            pltpu.VMEM((2 * width, 2 * hidden_width), bf16),
+            pltpu.VMEM((hidden_width, 2 * width), bf16),
+            pltpu.VMEM((2, tok_rows, 128), f32),
+            pltpu.VMEM((2, tok_rows, 128), f32),
+            pltpu.VMEM((tok_rows, width), f32),
+            pltpu.SemaphoreType.DMA((3,)),
+            pltpu.SemaphoreType.DMA((2,)),
+            pltpu.SemaphoreType.DMA((2,)),
+        ]
+        + lines,
+        compiler_params=pltpu.CompilerParams(
+            collective_id=0, has_side_effects=True, vmem_limit_bytes=60 * 1024 * 1024
+        ),
+    )(
+        tokens,
+        own_gain_in,
+        own_gain_out,
+        expert_ids.T,
+        route_weight.T,
+        gate_weight,
+        up_weight,
+        down_weight,
+    )
+
+
 def solution(mesh):
     in_specs = (
         P(("grp", "ep"), "tp"),
@@ -78,4 +441,4 @@
         P("ep", "tp", None),
     )
     out_specs = P(("grp", "ep"), "tp")
-    return jax.shard_map(shards, mesh=mesh, in_specs=in_specs, out_specs=out_specs, check_vma=False)
+    return jax.shard_map(layer, mesh=mesh, in_specs=in_specs, out_specs=out_specs, check_vma=False)

time: 207 us -> 86 us (0.42)
  Pallas kernels: 0 us -> 81.2 us
  waiting for transfers between devices: 81 us -> 0 us
  blocking collectives: 66.3 us -> 0 us
  matrix products: 21.7 us -> 0 us
  between operations: 13.6 us -> 0.01 us
  other arithmetic: 10 us -> 0 us
  starting transfers between devices: 5.94 us -> 0 us
  local copies, waits for them, and re-layouts: 7.8 us -> 4.32 us
    pallas_call x0 -> x1, Pallas kernels: none -> 81.2 us  [layer(): pl.pallas_call(functools.partial(fused, experts, cap), out_shape=jax.Shap...]
    all_to_all x1 -> x0, blocking collectives: 61.2 us -> none  [shards(): lax.all_to_all(outgoing, 'ep', split_axis=0, concat_axis=0, tiled=True)]
    all_to_all x1 -> x0, waiting for transfers between devices: 53.6 us -> none  [shards(): lax.all_to_all(half_sum.astype(jnp.bfloat16), 'ep', split_axis=0, concat_...]
    dot_general x4 -> x0, matrix products: 21.7 us -> none  [the longest x1 8.11 us: shards(): jnp.dot(gathered, gate_weight[0], preferred_element_type=jnp.float32)]
    reduce_scatter x1 -> x0, waiting for transfers between devices: 13.7 us -> none  [shards(): lax.psum_scatter(partial_value, 'tp', scatter_dimension=2, tiled=True)]
    all_gather x1 -> x0, waiting for transfers between devices: 13.6 us -> none  [shards(): arrived = lax.all_gather(arrived, 'tp', axis=2, tiled=True)]
    reduce_sum x5 -> x0, other arithmetic: 6.9 us -> none  [the longest x1 3.12 us: shards(): routed = jnp.sum(picked * route_weight[:, :, None], axis=1)]
    all_to_all x1 -> x0, starting transfers between devices: 5.9 us -> none  [shards(): lax.all_to_all(half_sum.astype(jnp.bfloat16), 'ep', split_axis=0, concat_...]
  transfers between devices with their start and end apart: 3 -> 0, of which waited for: 3 -> 0; matrix products, arithmetic and copies ran while one was open for 0% -> 0% of each run, Pallas kernels for 0% -> 0%
where the time goes in v1:
time: 86 us; the launch traced here: 85.5 us
  Pallas kernels  81.2 us (94%)
  local copies, waits for them, and re-layouts  4.32 us (5%)
    pallas_call x1, Pallas kernels, layer(): pl.pallas_call(functools.partial(fused, experts, cap), out_shape=jax.Shap...  81.2 us
    unnamed x1, local copies, waits for them, and re-layouts  1.77 us

profile of v1, /device:TPU:0, one launch (start us, length us, event | category | flops | bytes accessed | tf_op | source)
XLA Modules:
  0.0 85.5 jit_solution(10956990752097612008)
XLA Ops:
  0.0 1.3 %dynamic_slice.6 = f32[1024]{0:T(1024)} dynamic-slice(f32[2048]{0:T(1024)} %param.9, s32[]{:T(128)S(6)} %select_n.4), dynamic_slice_sizes={1024} | dynamic-slice | bytes 8196 | tf_op jit(solution)/shard_map/dynamic_slice | solution.py:386
  1.3 1.3 %dynamic_slice.7 = f32[1024]{0:T(1024)} dynamic-slice(f32[2048]{0:T(1024)} %param.10, s32[]{:T(128)S(6)} %select_n.4), dynamic_slice_sizes={1024} | dynamic-slice | bytes 8196 | tf_op jit(solution)/shard_map/dynamic_slice | solution.py:387
  2.6 81.2 %shard_map.82 = bf16[192,1024]{1,0:T(8,128)(2,1)} custom-call(bf16[192,1024]{1,0:T(8,128)(2,1)} %tok_ref.1, f32[1,1024]{1,0:T(1,128)} %bitcast.4, f32[1,1024]{1,0:T(1,128)} %bitcast.5, s32[2,192]{1,0:T(2,128)} %bitcast.6, f32[2,192]{1,0:T(2,128)} %bitcast.7, bf16[1,2048,896]{2,1,0:T(8,128)(2,1)} %gate_hbm.1, bf16[1,2048,896]{2,1,0:T(8,128)(2,1)} %up_hbm.1, ...), custom_call_target="tpu_custom_call" | custom-call | tf_op jit(solution)/shard_map/pallas_call | solution.py:392
  83.8 1.8 %copy.10 = bf16[192,1024]{1,0:T(8,128)(2,1)} copy(bf16[192,1024]{1,0:T(8,128)(2,1)} %shard_map.82) | data formatting | bytes 786432

commit v2 on v1

--- a/solution.py
+++ b/solution.py
@@ -128,6 +128,13 @@
     own_cols = pl.ds(pl.multiple_of(core * width, 128), width)
     other_cols = pl.ds(pl.multiple_of(other * width, 128), width)
 
+    way = 1 - 2 * (2 * mine // experts)
+    near = mine * (1 + way) // 2 + (experts - 1 - mine) * (1 - way) // 2
+
+    def nearest(turn):
+        both = jnp.where(turn % 2 == 1, -way, way) * ((turn + 1) // 2)
+        return (jnp.where(turn <= 2 * near, both, way * (turn - near)) + experts) % experts
+
     def on_line(step):
         return 2 * ((mine + step) % experts) + half
 
@@ -246,7 +253,7 @@
     sum_copy(0).wait_recv()
     squares = sums[0] + peer_sums[0]
     factor = lax.rsqrt(squares[:, 0:1] / (2 * width) + norm_eps)
-    normed = (own_float * factor * gain_in_ref[...]).astype(jnp.bfloat16)
+    normed = (own_float * factor * gain_in_ref[:, own_cols]).astype(jnp.bfloat16)
 
     def pack(step):
         one, two = hits(step)
@@ -256,7 +263,8 @@
     rows[0, 0, :, own_cols] = pack(0)
     pair_copy(0).start()
     core_copy(0).start()
-    for step in range(experts - 1, 0, -1):
+    for turn in range(1, experts):
+        step = nearest(turn)
         packed[step] = pack(step)
         line_copy(step).start()
 
@@ -296,37 +304,41 @@
         cross_copy(d).wait_recv()
         return (kept[d] + crossed[d].astype(jnp.float32)).astype(jnp.bfloat16)
 
+    relay_line(nearest(1))
     relay_pair(0)
     for load in loads:
         load.wait()
 
-    def step_of(d, carry):
-        @pl.when(d + 1 < experts)
+    def step_of(turn, carry):
+        d = nearest(turn)
+        compute(d)
+
+        @pl.when((turn > 0) & (turn + 1 < experts))
         def _():
-            relay_line(d + 1)
-
-        compute(d)
-
-        @pl.when(d + 1 < experts)
-        def _():
-            relay_pair(d + 1)
+            relay_line(nearest(turn + 1))
 
         cross(d)
 
-        @pl.when(d == 1)
+        @pl.when(turn == 1)
         def _():
             home[0] = send_home(0)
 
-        @pl.when(d > 1)
+        @pl.when(turn > 1)
         def _():
-            leaving[d - 1] = send_home(d - 1)
-            home_copy(d - 1).start()
+            last = nearest(turn - 1)
+            leaving[last] = send_home(last)
+            home_copy(last).start()
+
+        @pl.when(turn + 1 < experts)
+        def _():
+            relay_pair(nearest(turn + 1))
 
         return carry
 
     lax.fori_loop(0, experts, step_of, 0)
-    leaving[experts - 1] = send_home(experts - 1)
-    home_copy(experts - 1).start()
+    final = nearest(experts - 1)
+    leaving[final] = send_home(final)
+    home_copy(final).start()
 
     def combine(step):
         one, two = hits(step)
@@ -339,7 +351,8 @@
         ) + lax.dot_general(low, home[step], dims, preferred_element_type=jnp.float32)
 
     total[...] = combine(0)
-    for step in range(experts - 1, 0, -1):
+    for turn in range(1, experts):
+        step = nearest(turn)
         home_copy(experts - step).wait_recv()
         total[...] += combine(step)
     routed = total[...]
@@ -348,7 +361,7 @@
     sum_copy(1).wait_recv()
     squares_out = sums[1] + peer_sums[1]
     factor_out = lax.rsqrt(squares_out[:, 0:1] / (2 * width) + norm_eps)
-    out_ref[...] = (total[...] * factor_out * gain_out_ref[...]).astype(jnp.bfloat16)
+    out_ref[...] = (total[...] * factor_out * gain_out_ref[:, own_cols]).astype(jnp.bfloat16)
 
     sum_copy(0).wait_send()
     sum_copy(1).wait_send()
@@ -382,9 +395,6 @@
         return plain(
             tokens, gain_in, gain_out, expert_ids, route_weight, gate_weight, up_weight, down_weight
         )
-    own = lax.axis_index("tp") * width
-    own_gain_in = lax.dynamic_slice_in_dim(gain_in, own, width)[None, :]
-    own_gain_out = lax.dynamic_slice_in_dim(gain_out, own, width)[None, :]
     vmem = pl.BlockSpec(memory_space=pltpu.VMEM)
     hbm = pl.BlockSpec(memory_space=pl.ANY)
     bf16, f32 = jnp.bfloat16, jnp.float32
@@ -419,8 +429,8 @@
         ),
     )(
         tokens,
-        own_gain_in,
-        own_gain_out,
+        gain_in[None, :],
+        gain_out[None, :],
         expert_ids.T,
         route_weight.T,
         gate_weight,

time: 86 us -> 91.4 us (1.063)
  Pallas kernels: 81.2 us -> 89.4 us
  local copies, waits for them, and re-layouts: 4.32 us -> 1.77 us
    pallas_call x1, Pallas kernels: 81.2 us -> 89.4 us  [layer(): pl.pallas_call(functools.partial(fused, experts, cap), out_shape=jax.Shap...]
    dynamic_slice x2 -> x0, local copies, waits for them, and re-layouts: 2.55 us -> none  [the longest x1 1.28 us: layer(): own_gain_in = lax.dynamic_slice_in_dim(gain_in, own, width)[None, :]]
where the time goes in v2:
time: 91.4 us; the launch traced here: 91.2 us
  Pallas kernels  89.4 us (98%)
  local copies, waits for them, and re-layouts  1.77 us (2%)
    pallas_call x1, Pallas kernels, layer(): pl.pallas_call(functools.partial(fused, experts, cap), out_shape=jax.Shap...  89.4 us

profile of v2, /device:TPU:0, one launch (start us, length us, event | category | flops | bytes accessed | tf_op | source)
XLA Modules:
  0.0 91.2 jit_solution(6907924092104069072)
XLA Ops:
  0.0 89.4 %shard_map.82 = bf16[192,1024]{1,0:T(8,128)(2,1)} custom-call(bf16[192,1024]{1,0:T(8,128)(2,1)} %tok_ref.1, f32[1,2048]{1,0:T(1,128)} %bitcast.4, f32[1,2048]{1,0:T(1,128)} %bitcast.5, s32[2,192]{1,0:T(2,128)} %bitcast.6, f32[2,192]{1,0:T(2,128)} %bitcast.7, bf16[1,2048,896]{2,1,0:T(8,128)(2,1)} %gate_hbm.1, bf16[1,2048,896]{2,1,0:T(8,128)(2,1)} %up_hbm.1, ...), custom_call_target="tpu_custom_call" | custom-call | tf_op jit(solution)/shard_map/pallas_call | solution.py:402
  89.4 1.8 %copy.10 = bf16[192,1024]{1,0:T(8,128)(2,1)} copy(bf16[192,1024]{1,0:T(8,128)(2,1)} %shard_map.82) | data formatting | bytes 786432

commit v3 on v1

--- a/solution.py
+++ b/solution.py
@@ -71,6 +71,7 @@
 
 
 MESH = pl.DeviceIdType.MESH
+pieces = 2
 
 
 def fused(
@@ -128,6 +129,14 @@
     own_cols = pl.ds(pl.multiple_of(core * width, 128), width)
     other_cols = pl.ds(pl.multiple_of(other * width, 128), width)
 
+    piece = width // pieces
+
+    def cut(s):
+        return pl.ds(s * piece, piece)
+
+    def of_core(which, s):
+        return pl.ds(pl.multiple_of(which * width + s * piece, 128), piece)
+
     def on_line(step):
         return 2 * ((mine + step) % experts) + half
 
@@ -161,40 +170,32 @@
             sums.at[which], peer_sums.at[which], sq_send.at[which], sq_recv.at[which], {"tp": other}
         )
 
-    def line_copy(step):
+    def line_copy(step, s):
         back = experts - step
         return remote(
-            packed.at[step],
-            rows.at[back, 0, :, own_cols],
-            line_send.at[back],
-            line_recv.at[back],
+            packed.at[step, :, cut(s)],
+            rows.at[back, 0, :, of_core(core, s)],
+            line_send.at[back * pieces + s],
+            line_recv.at[back * pieces + s],
             {"ep": on_line(step)},
         )
 
-    def core_copy(d):
-        view = rows.at[d, 0, :, own_cols]
-        return remote(view, view, core_send.at[d], core_recv.at[d], {"tp": other})
-
-    def core_arrival(d):
-        view = rows.at[d, 0, :, other_cols]
-        return remote(view, view, core_send.at[d], core_recv.at[d], {"tp": other})
-
-    def pair_copy(d):
-        return remote(
-            rows.at[d, 0, :, own_cols],
-            rows.at[d, 1, :, own_cols],
-            pair_send.at[d],
-            pair_recv.at[d],
+    def core_copy(d, s, which=core):
+        view, sem = rows.at[d, 0, :, of_core(which, s)], d * pieces + s
+        return remote(view, view, core_send.at[sem], core_recv.at[sem], {"tp": other})
+
+    def pair_copy(d, s):
+        return remote(
+            rows.at[d, 0, :, of_core(core, s)],
+            rows.at[d, 1, :, of_core(core, s)],
+            pair_send.at[d * pieces + s],
+            pair_recv.at[d * pieces + s],
             {"ep": partner},
         )
 
-    def relay_copy(d):
-        view = rows.at[d, 1, :, own_cols]
-        return remote(view, view, relay_send.at[d], relay_recv.at[d], {"tp": other})
-
-    def relay_arrival(d):
-        view = rows.at[d, 1, :, other_cols]
-        return remote(view, view, relay_send.at[d], relay_recv.at[d], {"tp": other})
+    def relay_copy(d, s, which=core):
+        view, sem = rows.at[d, 1, :, of_core(which, s)], d * pieces + s
+        return remote(view, view, relay_send.at[sem], relay_recv.at[sem], {"tp": other})
 
     def part_copy(d):
         return remote(
@@ -205,15 +206,25 @@
             {"tp": other},
         )
 
-    def cross_copy(d):
-        return remote(
-            crossing.at[d], crossed.at[d], cross_send.at[d], cross_recv.at[d], {"ep": partner}
-        )
-
-    def home_copy(d):
+    def cross_copy(d, s):
+        sem = d * pieces + s
+        return remote(
+            crossing.at[d, :, cut(s)],
+            crossed.at[d, :, cut(s)],
+            cross_send.at[sem],
+            cross_recv.at[sem],
+            {"ep": partner},
+        )
+
+    def home_copy(d, s):
         back = experts - d
-        return remote(
-            leaving.at[d], home.at[back], home_send.at[back], home_recv.at[back], {"ep": on_line(d)}
+        sem = back * pieces + s
+        return remote(
+            leaving.at[d, :, cut(s)],
+            home.at[back, :, cut(s)],
+            home_send.at[sem],
+            home_recv.at[sem],
+            {"ep": on_line(d)},
         )
 
     own_float = tok_ref[...].astype(jnp.float32)
@@ -246,7 +257,7 @@
     sum_copy(0).wait_recv()
     squares = sums[0] + peer_sums[0]
     factor = lax.rsqrt(squares[:, 0:1] / (2 * width) + norm_eps)
-    normed = (own_float * factor * gain_in_ref[...]).astype(jnp.bfloat16)
+    normed = (own_float * factor * gain_in_ref[:, own_cols]).astype(jnp.bfloat16)
 
     def pack(step):
         one, two = hits(step)
@@ -254,24 +265,29 @@
         return jnp.dot(placing, normed, preferred_element_type=jnp.float32).astype(jnp.bfloat16)
 
     rows[0, 0, :, own_cols] = pack(0)
-    pair_copy(0).start()
-    core_copy(0).start()
+    for s in range(pieces):
+        pair_copy(0, s).start()
+        core_copy(0, s).start()
     for step in range(experts - 1, 0, -1):
         packed[step] = pack(step)
-        line_copy(step).start()
+        for s in range(pieces):
+            line_copy(step, s).start()
 
     def relay_line(d):
-        line_copy(experts - d).wait_recv()
-        pair_copy(d).start()
-        core_copy(d).start()
+        for s in range(pieces):
+            line_copy(experts - d, s).wait_recv()
+            pair_copy(d, s).start()
+            core_copy(d, s).start()
 
     def relay_pair(d):
-        pair_copy(d).wait_recv()
-        relay_copy(d).start()
+        for s in range(pieces):
+            pair_copy(d, s).wait_recv()
+            relay_copy(d, s).start()
 
     def compute(d):
-        core_arrival(d).wait_recv()
-        relay_arrival(d).wait_recv()
+        for s in range(pieces):
+            core_copy(d, s, other).wait_recv()
+            relay_copy(d, s, other).wait_recv()
         block = rows[d].reshape(2 * cap, 2 * width)
         pre = jnp.dot(block, gate_up[...], preferred_element_type=jnp.float32)
         gate_pre = pre[:, :hidden_width]
@@ -284,17 +300,30 @@
 
     def cross(d):
         part_copy(d).wait_recv()
-        crossing[d] = (
-            parts[d, 1, :, own_cols].astype(jnp.float32) + peer_parts[d, 1].astype(jnp.float32)
-        ).astype(jnp.bfloat16)
-        cross_copy(d).start()
+        for s in range(pieces):
+            crossing[d, :, cut(s)] = (
+                parts[d, 1, :, of_core(core, s)].astype(jnp.float32)
+                + peer_parts[d, 1, :, cut(s)].astype(jnp.float32)
+            ).astype(jnp.bfloat16)
+            cross_copy(d, s).start()
         kept[d] = parts[d, 0, :, own_cols].astype(jnp.float32) + peer_parts[d, 0].astype(
             jnp.float32
         )
 
+    def meet(d, s):
+        cross_copy(d, s).wait_recv()
+        return (kept[d, :, cut(s)] + crossed[d, :, cut(s)].astype(jnp.float32)).astype(
+            jnp.bfloat16
+        )
+
+    def keep_own():
+        for s in range(pieces):
+            home[0, :, cut(s)] = meet(0, s)
+
     def send_home(d):
-        cross_copy(d).wait_recv()
-        return (kept[d] + crossed[d].astype(jnp.float32)).astype(jnp.bfloat16)
+        for s in range(pieces):
+            leaving[d, :, cut(s)] = meet(d, s)
+            home_copy(d, s).start()
 
     relay_pair(0)
     for load in loads:
@@ -315,55 +344,62 @@
 
         @pl.when(d == 1)
         def _():
-            home[0] = send_home(0)
+            keep_own()
 
         @pl.when(d > 1)
         def _():
-            leaving[d - 1] = send_home(d - 1)
-            home_copy(d - 1).start()
+            send_home(d - 1)
 
         return carry
 
     lax.fori_loop(0, experts, step_of, 0)
-    leaving[experts - 1] = send_home(experts - 1)
-    home_copy(experts - 1).start()
-
-    def combine(step):
+    send_home(experts - 1)
+
+    def weights_of(step):
         one, two = hits(step)
         mix = jnp.where(one, route_ref[0:1, :], 0.0) + jnp.where(two, route_ref[1:2, :], 0.0)
         high = mix.astype(jnp.bfloat16)
-        low = (mix - high.astype(jnp.float32)).astype(jnp.bfloat16)
+        return high, (mix - high.astype(jnp.float32)).astype(jnp.bfloat16)
+
+    def combine(step, s, high, low):
         dims = (((0,), (0,)), ((), ()))
+        values = home[step, :, cut(s)]
         return lax.dot_general(
-            high, home[step], dims, preferred_element_type=jnp.float32
-        ) + lax.dot_general(low, home[step], dims, preferred_element_type=jnp.float32)
-
-    total[...] = combine(0)
+            high, values, dims, preferred_element_type=jnp.float32
+        ) + lax.dot_general(low, values, dims, preferred_element_type=jnp.float32)
+
+    mixes = weights_of(0)
+    for s in range(pieces):
+        total[:, cut(s)] = combine(0, s, *mixes)
     for step in range(experts - 1, 0, -1):
-        home_copy(experts - step).wait_recv()
-        total[...] += combine(step)
+        mixes = weights_of(step)
+        for s in range(pieces):
+            home_copy(experts - step, s).wait_recv()
+            total[:, cut(s)] += combine(step, s, *mixes)
     routed = total[...]
     sums[1] = jnp.broadcast_to(jnp.sum(routed * routed, axis=1, keepdims=True), (tok_rows, 128))
     sum_copy(1).start()
     sum_copy(1).wait_recv()
     squares_out = sums[1] + peer_sums[1]
     factor_out = lax.rsqrt(squares_out[:, 0:1] / (2 * width) + norm_eps)
-    out_ref[...] = (total[...] * factor_out * gain_out_ref[...]).astype(jnp.bfloat16)
+    out_ref[...] = (total[...] * factor_out * gain_out_ref[:, own_cols]).astype(jnp.bfloat16)
 
     sum_copy(0).wait_send()
     sum_copy(1).wait_send()
 
     def drain(d, carry):
-        core_copy(d).wait_send()
-        pair_copy(d).wait_send()
-        relay_copy(d).wait_send()
+        for s in range(pieces):
+            core_copy(d, s).wait_send()
+            pair_copy(d, s).wait_send()
+            relay_copy(d, s).wait_send()
+            cross_copy(d, s).wait_send()
         part_copy(d).wait_send()
-        cross_copy(d).wait_send()
 
         @pl.when(d > 0)
         def _():
-            line_copy(d).wait_send()
-            home_copy(d).wait_send()
+            for s in range(pieces):
+                line_copy(d, s).wait_send()
+                home_copy(d, s).wait_send()
 
         return carry
 
@@ -378,17 +414,14 @@
     picks = expert_ids.shape[1]
     cap = tok_rows * picks * 3 // (2 * experts)
     hidden_width = gate_weight.shape[2]
-    if picks != 2 or experts < 2 or cap % 16 or width % 128 or hidden_width % 128:
+    if picks != 2 or experts < 2 or cap % 16 or width % (128 * pieces) or hidden_width % 128:
         return plain(
             tokens, gain_in, gain_out, expert_ids, route_weight, gate_weight, up_weight, down_weight
         )
-    own = lax.axis_index("tp") * width
-    own_gain_in = lax.dynamic_slice_in_dim(gain_in, own, width)[None, :]
-    own_gain_out = lax.dynamic_slice_in_dim(gain_out, own, width)[None, :]
     vmem = pl.BlockSpec(memory_space=pltpu.VMEM)
     hbm = pl.BlockSpec(memory_space=pl.ANY)
     bf16, f32 = jnp.bfloat16, jnp.float32
-    lines = [pltpu.SemaphoreType.DMA((experts,))] * 14
+    lines = [pltpu.SemaphoreType.DMA((experts * pieces,))] * 14
     return pl.pallas_call(
         functools.partial(fused, experts, cap),
         out_shape=jax.ShapeDtypeStruct((tok_rows, width), bf16),
@@ -419,8 +452,8 @@
         ),
     )(
         tokens,
-        own_gain_in,
-        own_gain_out,
+        gain_in[None, :],
+        gain_out[None, :],
         expert_ids.T,
         route_weight.T,
         gate_weight,

time: 86 us -> 82.9 us (0.964)
  local copies, waits for them, and re-layouts: 4.32 us -> 1.77 us
  Pallas kernels: 81.2 us -> 80.2 us
    dynamic_slice x2 -> x0, local copies, waits for them, and re-layouts: 2.55 us -> none  [the longest x1 1.28 us: layer(): own_gain_in = lax.dynamic_slice_in_dim(gain_in, own, width)[None, :]]
    pallas_call x1, Pallas kernels: 81.2 us -> 80.2 us  [layer(): pl.pallas_call(functools.partial(fused, experts, cap), out_shape=jax.Shap...]
where the time goes in v3:
time: 82.9 us; the launch traced here: 81.9 us
  Pallas kernels  80.2 us (97%)
  local copies, waits for them, and re-layouts  1.77 us (2%)
    pallas_call x1, Pallas kernels, layer(): pl.pallas_call(functools.partial(fused, experts, cap), out_shape=jax.Shap...  80.2 us
    unnamed x1, local copies, waits for them, and re-layouts  1.77 us

profile of v3, /device:TPU:0, one launch (start us, length us, event | category | flops | bytes accessed | tf_op | source)
XLA Modules:
  0.0 81.9 jit_solution(8321422477063104506)
XLA Ops:
  0.0 80.2 %shard_map.82 = bf16[192,1024]{1,0:T(8,128)(2,1)} custom-call(bf16[192,1024]{1,0:T(8,128)(2,1)} %tok_ref.1, f32[1,2048]{1,0:T(1,128)} %bitcast.4, f32[1,2048]{1,0:T(1,128)} %bitcast.5, s32[2,192]{1,0:T(2,128)} %bitcast.6, f32[2,192]{1,0:T(2,128)} %bitcast.7, bf16[1,2048,896]{2,1,0:T(8,128)(2,1)} %gate_hbm.1, bf16[1,2048,896]{2,1,0:T(8,128)(2,1)} %up_hbm.1, ...), custom_call_target="tpu_custom_call" | custom-call | tf_op jit(solution)/shard_map/pallas_call | solution.py:425
  80.2 1.8 %copy.10 = bf16[192,1024]{1,0:T(8,128)(2,1)} copy(bf16[192,1024]{1,0:T(8,128)(2,1)} %shard_map.82) | data formatting | bytes 786432

commit v4 on v3

--- a/solution.py
+++ b/solution.py
@@ -335,20 +335,19 @@
             relay_line(d + 1)
 
         compute(d)
+        cross(d)
+
+        @pl.when(d == 1)
+        def _():
+            keep_own()
+
+        @pl.when(d > 1)
+        def _():
+            send_home(d - 1)
 
         @pl.when(d + 1 < experts)
         def _():
             relay_pair(d + 1)
-
-        cross(d)
-
-        @pl.when(d == 1)
-        def _():
-            keep_own()
-
-        @pl.when(d > 1)
-        def _():
-            send_home(d - 1)
 
         return carry
 

time: 82.9 us -> 80.6 us (0.972)
  Pallas kernels: 80.2 us -> 77.6 us
    pallas_call x1, Pallas kernels: 80.2 us -> 77.6 us  [layer(): pl.pallas_call(functools.partial(fused, experts, cap), out_shape=jax.Shap...]
where the time goes in v4:
time: 80.6 us; the launch traced here: 79.4 us
  Pallas kernels  77.6 us (96%)
  local copies, waits for them, and re-layouts  1.77 us (2%)
    pallas_call x1, Pallas kernels, layer(): pl.pallas_call(functools.partial(fused, experts, cap), out_shape=jax.Shap...  77.6 us
    unnamed x1, local copies, waits for them, and re-layouts  1.77 us

profile of v4, /device:TPU:0, one launch (start us, length us, event | category | flops | bytes accessed | tf_op | source)
XLA Modules:
  0.0 79.4 jit_solution(527447829598808659)
XLA Ops:
  0.0 77.6 %shard_map.82 = bf16[192,1024]{1,0:T(8,128)(2,1)} custom-call(bf16[192,1024]{1,0:T(8,128)(2,1)} %tok_ref.1, f32[1,2048]{1,0:T(1,128)} %bitcast.4, f32[1,2048]{1,0:T(1,128)} %bitcast.5, s32[2,192]{1,0:T(2,128)} %bitcast.6, f32[2,192]{1,0:T(2,128)} %bitcast.7, bf16[1,2048,896]{2,1,0:T(8,128)(2,1)} %gate_hbm.1, bf16[1,2048,896]{2,1,0:T(8,128)(2,1)} %up_hbm.1, ...), custom_call_target="tpu_custom_call" | custom-call | tf_op jit(solution)/shard_map/pallas_call | solution.py:424
  77.6 1.8 %copy.10 = bf16[192,1024]{1,0:T(8,128)(2,1)} copy(bf16[192,1024]{1,0:T(8,128)(2,1)} %shard_map.82) | data formatting | bytes 786432
